TPU v7x, 512 devices: a whole 4x4x16 slice. The times are simulated.
512 devices in a mesh: sp: 128 (over z, x, core), tp: 4 (over y).
Axes of the slice: x: 4, y: 4, z: 16, core: 2. Of those that a mesh axis runs over, the one named last changes fastest.
Arguments:
- inputs: bfloat16 [4, 16384, 1024], P(None, 'sp'), may hold values from -6 to 6
- norm_gain: float32 [1024], replicated, may hold values from 0.1 to 1.9
- query_weight: bfloat16 [1024, 3, 8, 64], P('sp', None, 'tp'), may hold values from -0.1875 to 0.1875
- key_weight: bfloat16 [1024, 3, 8, 64], P('sp', None, 'tp'), may hold values from -0.1875 to 0.1875
- value_weight: bfloat16 [1024, 3, 8, 64], P('sp', None, 'tp'), may hold values from -0.1875 to 0.1875
- query_gain: float32 [3, 64], replicated, may hold values from 0.1 to 1.9
- key_gain: float32 [3, 64], replicated, may hold values from 0.1 to 1.9
- out_weight: bfloat16 [8, 64, 1024], P('tp', None, 'sp'), may hold values from -0.75 to 0.75
Outputs:
- mixed: bfloat16 [4, 16384, 1024], P(None, 'sp', 'tp')
All inputs are finite; a program needn't handle non-finite values.
Results may differ from a plain program's by a relative error of at most 0.02.
Values may be sent and summed in bfloat16 or wider, within the bound.
A program may use at most 64 MiB of HBM per device.

v0:
```python
import math
import jax
import jax.numpy as jnp
from jax import lax
from jax.sharding import Mesh
from jax.sharding import PartitionSpec as P

SPAN_CLOSE = 32
SPREAD_CENTRAL = 4
SPAN_CENTRAL = 32
SPREAD_DISTANT = 16
SPAN_DISTANT = 16
SP = ("sp_0", "sp_1", "sp_2")
eps = 1e-06
neg_fill = -1e30


def joined_along(tiles, dim):
    tiles = jnp.moveaxis(tiles, 0, dim)
    shape = tiles.shape
    return tiles.reshape(*shape[:dim], shape[dim] * shape[dim + 1], *shape[dim + 2 :])


def stacked_from(value, axes, sequence):
    tiles = value[None]
    for k in sequence:
        tiles = lax.all_gather(tiles, axes[k], axis=0, tiled=True)
    block = [lax.axis_size(axes[k]) for k in reversed(sequence)]
    tiles = tiles.reshape(*block, *value.shape)
    turned = sorted(range(len(sequence)), key=lambda place: sequence[len(sequence) - 1 - place])
    return tiles.transpose(*turned, *range(len(sequence), tiles.ndim)).reshape(-1, *value.shape)


def gather_axes(value, axes, sequence, dim):
    return joined_along(stacked_from(value, axes, sequence), dim)


def over_axes(value, axes, sequence, dim, take_in, carry):
    everything = jax.tree.map(lambda part: gather_axes(part, axes, sequence, dim), value)
    return take_in(carry, everything, jnp.int32(0))


def padded(cells, sides, width, closed):
    for axis, dim in sides:
        count = lax.axis_size(axis)
        ends = count if closed else count - 1
        head = lax.slice_in_dim(cells, 0, width, axis=dim)
        tail = lax.slice_in_dim(cells, cells.shape[dim] - width, cells.shape[dim], axis=dim)
        cells = jnp.concatenate(
            [
                lax.ppermute(tail, axis, [(i, (i + 1) % count) for i in range(ends)]),
                cells,
                lax.ppermute(head, axis, [((i + 1) % count, i) for i in range(ends)]),
            ],
            axis=dim,
        )
    return cells


def shifted(block, axis, distance):
    devices = range(lax.axis_size(axis))
    route = [(i - distance, i) for i in devices if i - distance in devices]
    return lax.ppermute(block, axis, route)


def on_whole(value, axes, sequence, dim, apply):
    return apply(gather_axes(value, axes, sequence, dim), jnp.int32(0))


def row_norm(values, gain):
    scaled = values * lax.rsqrt(jnp.mean(values * values, axis=-1, keepdims=True) + eps)
    return scaled * gain


def band_attend(queries, keys, values, margin, dilation, half, slopes, anchor, seq_len):
    batch, count, heads, width = queries.shape
    query_rows = count // dilation
    key_rows = query_rows + 2 * half
    first = margin - half * dilation
    keys = keys[:, first : first + key_rows * dilation]
    values = values[:, first : first + key_rows * dilation]
    query_sub = queries.reshape(batch, query_rows, dilation, heads, width)
    key_sub = keys.reshape(batch, key_rows, dilation, heads, width)
    value_sub = values.reshape(batch, key_rows, dilation, heads, width)
    scores = jnp.einsum(
        "barhe,bcrhe->brhac", query_sub, key_sub, precision=lax.Precision.DEFAULT
    ) / math.sqrt(width)
    offset = jnp.arange(key_rows)[None, :] - half - jnp.arange(query_rows)[:, None]
    key_place = (
        anchor + first + dilation * jnp.arange(key_rows)[None, :] + jnp.arange(dilation)[:, None]
    )
    inside = (key_place >= 0) & (key_place < seq_len)
    allowed = (jnp.abs(offset) <= half)[None, :, :] & inside[:, None, :]
    slant = -slopes[:, None, None] * (jnp.abs(offset).astype(jnp.float32) / float(half))[None]
    scores = jnp.where(allowed[None, :, None], scores + slant[None, None], neg_fill)
    log_total = jax.nn.logsumexp(scores, axis=-1)
    weights = jnp.exp(scores - log_total[..., None])
    result = jnp.einsum("brhac,bcrhe->barhe", weights, value_sub, precision=lax.Precision.DEFAULT)
    log_total = jnp.transpose(log_total, (0, 3, 1, 2)).reshape(batch, count, heads)
    return (result.reshape(batch, count, heads, width), log_total)


def assemble(own, fetched, reach):
    before = [fetched[distance] for distance in range(reach, 0, -1)]
    after = [fetched[-distance] for distance in range(1, reach + 1)]
    return jnp.concatenate(before + [own] + after, axis=1)


def body(
    inputs, norm_gain, query_weight, key_weight, value_weight, query_gain, key_gain, out_weight
):
    batch, local_sequence_count, model_width = inputs.shape
    groups = query_weight.shape[1]
    heads_here = query_weight.shape[2]
    head_width = query_weight.shape[3]
    seq_len = local_sequence_count * lax.axis_size(SP)
    place = lax.axis_index(SP) * local_sequence_count
    flat = inputs.reshape(batch * local_sequence_count, model_width).astype(jnp.float32)
    normed = row_norm(flat, norm_gain).astype(jnp.bfloat16)
    empty = jnp.zeros((batch * local_sequence_count, groups * heads_here * head_width), jnp.float32)

    def add_rows(totals, pieces, start):
        rows = pieces[0].shape[0]
        columns = lax.dynamic_slice_in_dim(normed, start, rows, 1)
        return tuple(
            (
                total
                + jnp.dot(columns, piece.reshape(rows, -1), preferred_element_type=jnp.float32)
                for total, piece in zip(totals, pieces)
            )
        )

    projected = over_axes(
        (query_weight, key_weight, value_weight),
        (("sp_0", "sp_1"), "sp_2"),
        (0, 1),
        0,
        add_rows,
        (empty, empty, empty),
    )
    layout = (batch, local_sequence_count, groups, heads_here, head_width)
    queries = projected[0].astype(jnp.bfloat16).reshape(layout)
    keys = projected[1].astype(jnp.bfloat16).reshape(layout)
    values = projected[2].astype(jnp.bfloat16).reshape(layout)
    pairs = jnp.concatenate([keys, values], axis=-1)
    total_heads = heads_here * lax.axis_size("tp")
    head_index = lax.axis_index("tp") * heads_here + jnp.arange(heads_here)
    slopes = jnp.exp2(-8.0 * (head_index + 1).astype(jnp.float32) / total_heads)
    central_extent = (
        SPREAD_CENTRAL * SPAN_CENTRAL + local_sequence_count - 1
    ) // local_sequence_count
    distant_extent = (
        SPREAD_DISTANT * SPAN_DISTANT + local_sequence_count - 1
    ) // local_sequence_count
    near_window = padded(pairs[:, :, 0], ((SP, 1),), SPAN_CLOSE, False)
    mid_fetched = {}
    far_fetched = {}
    for distance in range(1, central_extent + 1):
        for direction in (1, -1):
            both = shifted(pairs[:, :, 1:], SP, direction * distance)
            mid_fetched[direction * distance] = both[:, :, 0]
            far_fetched[direction * distance] = both[:, :, 1]
    for distance in range(central_extent + 1, distant_extent + 1):
        for direction in (1, -1):
            far_fetched[direction * distance] = shifted(pairs[:, :, 2], SP, direction * distance)
    central_span_width = assemble(pairs[:, :, 1], mid_fetched, central_extent)
    distant_span_width = assemble(pairs[:, :, 2], far_fetched, distant_extent)
    settings = (
        (near_window, SPAN_CLOSE, 1, SPAN_CLOSE),
        (central_span_width, central_extent * local_sequence_count, SPREAD_CENTRAL, SPAN_CENTRAL),
        (distant_span_width, distant_extent * local_sequence_count, SPREAD_DISTANT, SPAN_DISTANT),
    )
    results = []
    totals = []
    for group in range(3):
        window, margin, dilation, half = settings[group]
        query_group = row_norm(queries[:, :, group].astype(jnp.float32), query_gain[group])
        key_group = row_norm(window[..., :head_width].astype(jnp.float32), key_gain[group])
        value_group = window[..., head_width:].astype(jnp.float32)
        result, log_total = band_attend(
            query_group,
            key_group,
            value_group,
            margin,
            dilation,
            half,
            slopes,
            place - margin,
            seq_len,
        )
        results.append(result)
        totals.append(log_total)
    weights = jax.nn.softmax(jnp.stack(totals, 0), axis=0)
    combined = jnp.sum(weights[..., None] * jnp.stack(results, 0), axis=0)
    merged = combined.astype(jnp.bfloat16).reshape(
        batch * local_sequence_count, heads_here * head_width
    )

    def project(piece, start):
        return jnp.dot(merged, piece, preferred_element_type=jnp.float32)

    terms = on_whole(out_weight.reshape(heads_here * head_width, -1), SP, (0, 1, 2), 1, project)
    summed = lax.psum_scatter(
        terms.astype(jnp.bfloat16), "tp", scatter_dimension=1, tiled=True
    ).astype(jnp.float32)
    return summed.astype(jnp.bfloat16).reshape(batch, local_sequence_count, -1)


def solution(mesh):
    finer = Mesh(mesh.devices.reshape(16, 4, 2, mesh.shape["tp"]), ("sp_0", "sp_1", "sp_2", "tp"))
    placed = (
        P(None, SP, None),
        P(),
        P(SP, None, "tp", None),
        P(SP, None, "tp", None),
        P(SP, None, "tp", None),
        P(),
        P(),
        P("tp", None, SP),
    )
    return jax.shard_map(
        body, mesh=finer, in_specs=placed, out_specs=P(None, SP, "tp"), check_vma=False
    )
```

profile of v0, /device:TPU:2, one launch (start us, length us, event | category | flops | bytes accessed | tf_op | source)
XLA Modules:
  0.0 474.6 jit_solution(8545988568318055102)
XLA Ops:
  6.5 1.5 fusion.2
  8.0 107.0 %all-gather.1 = bf16[512,3,2,64]{3,2,1,0:T(2,128)(2,1)S(1)} all-gather(bf16[8,3,2,64]{3,2,1,0:T(2,128)(2,1)} %param.11), channel_id=3, replica_groups=mesh['sp_0'=16,'sp_1'=4,'sp_2'=2,'tp'=4] {'sp_0','sp_1'}, dimensions={0}, use_global_device_ids=true | all-gather | bytes 399360 | tf_op jit(solution)/shard_map/all_gather | solution.py:27
  115.2 2.9 all_gather.30
  118.1 1.2 copy.329
  119.4 1.0 reshape_reshape_reshape.10
  120.4 98.5 %all-gather.2 = bf16[512,3,2,64]{3,2,1,0:T(2,128)(2,1)S(1)} all-gather(bf16[8,3,2,64]{3,2,1,0:T(2,128)(2,1)S(1)} %copy-done.10), channel_id=4, replica_groups=mesh['sp_0'=16,'sp_1'=4,'sp_2'=2,'tp'=4] {'sp_0','sp_1'}, dimensions={0}, use_global_device_ids=true | all-gather | bytes 399360 | tf_op jit(solution)/shard_map/all_gather | solution.py:27
  219.0 2.9 all_gather.32
  221.9 1.2 copy.328
  223.2 1.7 reshape_reshape_reshape.11
  225.3 0.8 copy-done.5
  226.1 0.7 convolution_convert_fusion.1
  226.8 0.7 convolution_convert_fusion.2
  227.9 1.0 copy.223
  229.3 1.0 copy.224
  230.4 0.8 fusion.57
  231.1 3.9 collective-permute-start.5
  235.1 2.0 collective-permute-start.4
  237.1 0.8 fusion.92
  237.9 2.0 collective-permute-start
  240.0 3.7 collective-permute-start.1
  243.6 0.8 fusion.43
  244.5 3.1 collective-permute-start.3
  247.6 0.6 fusion.84
  248.3 0.6 fusion.88
  248.9 0.5 slice_bitcast_fusion.9
  249.4 0.6 slice_bitcast_fusion.8
  250.1 0.7 broadcast_multiply_fusion.2
  250.7 0.7 broadcast_multiply_fusion.1
  251.5 0.7 fusion.71
  252.2 26.8 %all_gather.33 = bf16[16,128,8]{1,2,0:T(8,128)(2,1)S(1)} all-gather(bf16[1,128,8]{1,2,0:T(8,128)(2,1)S(1)} %broadcast_in_dim_reshape.3), channel_id=1, replica_groups=mesh['sp_0'=16,'sp_1'=4,'sp_2'=2,'tp'=4] {'sp_0'}, dimensions={0}, use_global_device_ids=true | all-gather | bytes 34816 | tf_op jit(solution)/shard_map/all_gather | solution.py:27
  279.1 0.8 broadcast_multiply_fusion
  279.8 14.0 %all_gather.34 = bf16[64,128,8]{1,2,0:T(8,128)(2,1)S(1)} all-gather(bf16[16,128,8]{1,2,0:T(8,128)(2,1)S(1)} %all_gather.33), channel_id=1, replica_groups=mesh['sp_0'=16,'sp_1'=4,'sp_2'=2,'tp'=4] {'sp_1'}, dimensions={0}, use_global_device_ids=true | all-gather | bytes 163840 | tf_op jit(solution)/shard_map/all_gather | solution.py:27
  293.8 98.9 %all-gather = bf16[512,3,2,64]{3,2,1,0:T(2,128)(2,1)S(1)} all-gather(bf16[8,3,2,64]{3,2,1,0:T(2,128)(2,1)S(1)} %copy-done.11), channel_id=2, replica_groups=mesh['sp_0'=16,'sp_1'=4,'sp_2'=2,'tp'=4] {'sp_0','sp_1'}, dimensions={0}, use_global_device_ids=true | all-gather | bytes 399360 | tf_op jit(solution)/shard_map/all_gather | solution.py:27
  392.9 3.1 all_gather.28
  396.0 1.2 copy.330
  397.2 1.7 reshape_reshape_reshape.9
  399.0 1.8 convolution_convert_fusion.3
  402.3 0.6 broadcast_and_fusion.1
  402.9 0.6 broadcast_and_fusion
  403.5 0.9 multiply_multiply_fusion
  404.4 1.0 multiply_multiply_fusion.1
  405.5 2.1 all_gather.35
  407.6 0.8 copy.260
  408.4 2.0 collective-permute-start.2
  410.4 1.3 pad_maximum_fusion.1
  411.9 0.4 fusion.95
  412.5 1.0 convolution_bitcast_fusion.1
  413.5 1.0 constant_dynamic-update-slice_fusion.2
  414.5 1.0 slice_bitcast_fusion.2
  415.5 4.4 collective-permute-done.2
  420.7 1.6 fusion.94
  422.7 0.6 fusion.78
  423.4 1.0 constant_dynamic-update-slice_fusion.1
  424.7 0.7 stack.13
  425.4 1.0 fusion.59
  426.4 1.0 constant_dynamic-update-slice_fusion
  427.7 0.9 fusion.8
  428.6 0.8 copy.239
  429.3 1.9 fusion.93
  431.4 0.5 exponential_reduce_fusion.1
  433.6 0.8 copy.252
  434.4 0.5 fusion.13
  436.1 1.5 convolution_convert_fusion
  437.5 30.2 %reduce-scatter.2.cloned.1.call-done = bf16[512,256]{1,0:T(8,128)(2,1)} async-done(((bf16[512,1024]{1,0:T(8,128)(2,1)}), bf16[512,256]{1,0:T(8,128)(2,1)}) %reduce-scatter.2.cloned.1.call-update) | async-done | bytes 262160 | tf_op jit(solution)/shard_map/reduce_scatter | solution.py:203
  (123 shorter events, 8.2 us)
Async XLA Ops:
  6.5 461.3 %reduce-scatter.2.cloned.1.call-start = ((), (), s32[]{:S(2)}) async-start(), calls=%async_computation.1 | async-start | bytes 1310720 | tf_op jit(solution)/shard_map/reduce_scatter | solution.py:203
  119.4 1.0 copy-start.10
  223.2 1.8 copy-start
  223.2 1.8 copy-start.12
  225.0 1.1 copy-start.5
  225.3 1.5 copy-start.2
  231.1 17.7 %copy-start.16 = (f32[3,64]{1,0:T(4,128)S(1)}, f32[3,64]{1,0:T(4,128)}, u32[]{:S(2)}) copy-start(f32[3,64]{1,0:T(4,128)} %param.13) | copy-start | bytes 2308
  231.1 18.3 %copy-start.17 = (f32[3,64]{1,0:T(4,128)S(1)}, f32[3,64]{1,0:T(4,128)}, u32[]{:S(2)}) copy-start(f32[3,64]{1,0:T(4,128)} %param.14) | copy-start | bytes 2308
  231.1 18.8 %copy-start.13 = (bf16[2,64,8]{1,2,0:T(8,128)(2,1)S(1)}, bf16[2,64,8]{1,2,0:T(8,128)(2,1)}, u32[]{:S(2)}) copy-start(bf16[2,64,8]{1,2,0:T(8,128)(2,1)} %param.15) | copy-start | bytes 6148
  231.1 195.3 %collective-permute-start.5 = (bf16[4,128,2,128]{1,3,2,0:T(8,128)(2,1)}, bf16[4,128,2,128]{1,3,2,0:T(8,128)(2,1)}, u32[]{:S(2)}, u32[]{:S(2)}) collective-permute-start(bf16[4,128,2,128]{1,3,2,0:T(8,128)(2,1)} %get-tuple-element.13), channel_id=1, source_target_pairs={{8,0},{12,4},{16,8},{20,12},{24,16},{28,20},{32,24},{36,28},{40,32... | collective-permute-start | bytes 786440 | tf_op jit(solution)/shard_map/ppermute | solution.py:63
  235.1 178.4 %collective-permute-start.4 = (bf16[4,128,2,128]{1,3,2,0:T(8,128)(2,1)}, bf16[4,128,2,128]{1,3,2,0:T(8,128)(2,1)}, u32[]{:S(2)}, u32[]{:S(2)}) collective-permute-start(bf16[4,128,2,128]{1,3,2,0:T(8,128)(2,1)} %get-tuple-element.13), channel_id=1, source_target_pairs={{0,8},{4,12},{8,16},{12,20},{16,24},{20,28},{24,32},{28,36},{32,40... | collective-permute-start | bytes 786440 | tf_op jit(solution)/shard_map/ppermute | solution.py:63
  237.9 55.9 %copy-start.11 = (bf16[8,3,2,64]{3,2,1,0:T(2,128)(2,1)S(1)}, bf16[8,3,2,64]{3,2,1,0:T(2,128)(2,1)}, u32[]{:S(2)}) copy-start(bf16[8,3,2,64]{3,2,1,0:T(2,128)(2,1)} %param.10) | copy-start | bytes 18436
  237.9 170.5 %collective-permute-start = (bf16[4,32,2,128]{1,3,2,0:T(8,128)(2,1)S(1)}, bf16[4,32,2,128]{1,3,2,0:T(8,128)(2,1)}, u32[]{:S(2)}, u32[]{:S(2)}) collective-permute-start(bf16[4,32,2,128]{1,3,2,0:T(8,128)(2,1)S(1)} %get-tuple-element.20), channel_id=1, source_target_pairs={{0,4},{4,8},{8,12},{12,16},{16,20},{20,24},{24,28},{28,32},{32,36}... | collective-permute-start | bytes 196616 | tf_op jit(solution)/shard_map/ppermute | solution.py:51
  240.0 170.5 %collective-permute-start.1 = (bf16[4,32,2,128]{1,3,2,0:T(8,128)(2,1)}, bf16[4,32,2,128]{1,3,2,0:T(8,128)(2,1)}, u32[]{:S(2)}, u32[]{:S(2)}) collective-permute-start(bf16[4,32,2,128]{1,3,2,0:T(8,128)(2,1)} %get-tuple-element.21), channel_id=1, source_target_pairs={{4,0},{8,4},{12,8},{16,12},{20,16},{24,20},{28,24},{32,28},{36,32}... | collective-permute-start | bytes 196616 | tf_op jit(solution)/shard_map/ppermute | solution.py:53
  244.5 170.0 %collective-permute-start.3 = (bf16[4,128,2,2,128]{1,4,3,0,2:T(8,128)(2,1)}, bf16[4,128,2,2,128]{1,4,3,0,2:T(8,128)(2,1)}, u32[]{:S(2)}, u32[]{:S(2)}) collective-permute-start(bf16[4,128,2,2,128]{1,4,3,0,2:T(8,128)(2,1)} %fusion.43), channel_id=1, source_target_pairs={{4,0},{8,4},{12,8},{16,12},{20,16},{24,20},{28,24},{32,28},{36,32}... | collective-permute-start | bytes 1572872 | tf_op jit(solution)/shard_map/ppermute | solution.py:63
  397.2 1.8 copy-start.3
  400.8 0.8 copy-start.14
  401.6 0.7 copy-start.20
  401.7 1.3 copy-start.18
  401.7 1.9 copy-start.15
  405.5 6.4 %copy-start.6 = (f32[2,128,192]{1,2,0:T(8,128)S(1)}, f32[2,128,192]{1,2,0:T(8,128)}, u32[]{:S(2)}) copy-start(f32[2,128,192]{1,2,0:T(8,128)} %broadcast_multiply_fusion) | copy-start | bytes 589828
  405.5 6.4 %copy-start.8 = (pred[128,192]{0,1:T(8,128)(4,1)S(1)}, pred[128,192]{0,1:T(8,128)(4,1)}, u32[]{:S(2)}) copy-start(pred[128,192]{0,1:T(8,128)(4,1)} %fusion.71) | copy-start | bytes 73732
  405.5 6.4 %copy-start.19 = (f32[64]{0:T(128)S(1)}, f32[64]{0:T(128)}, u32[]{:S(2)}) copy-start(f32[64]{0:T(128)} %get-tuple-element.22) | copy-start | bytes 772
  408.4 11.5 %collective-permute-start.2 = (bf16[4,128,2,2,128]{1,4,3,0,2:T(8,128)(2,1)}, bf16[4,128,2,2,128]{1,4,3,0,2:T(8,128)(2,1)S(1)}, u32[]{:S(2)}, u32[]{:S(2)}) collective-permute-start(bf16[4,128,2,2,128]{1,4,3,0,2:T(8,128)(2,1)} %fusion.43), channel_id=1, source_target_pairs={{0,4},{4,8},{8,12},{12,16},{16,20},{20,24},{24,28},{28,32},{32,36}... | collective-permute-start | bytes 1572872 | tf_op jit(solution)/shard_map/ppermute | solution.py:63
  429.3 2.9 copy-start.7
  434.9 0.7 copy-start.9
  434.9 1.0 copy-start.1
  434.9 1.1 copy-start.4
Sparse Core Ops, SparseCore 0:
  437.7 30.0 reduce-scatter.1
where the time goes:
time: 475 us
  blocking collectives  356 us (75%)
  waiting for transfers between devices  34.6 us (7%)
  local copies, waits for them, and re-layouts  26.4 us (6%)
  starting transfers between devices  16.8 us (4%)
  other arithmetic  15.9 us (3%)
  between operations  14.2 us (3%)
  matrix products  10.5 us (2%)
    all_gather x9, blocking collectives, stacked_from(): tiles = lax.all_gather(tiles, axes[k], axis=0, tiled=True)  356 us
    reduce_scatter x1, waiting for transfers between devices, body(): lax.psum_scatter(terms.astype(jnp.bfloat16), 'tp', scatter_dimension=1, t...  30.2 us
    ppermute x4, starting transfers between devices, shifted(): return lax.ppermute(block, axis, route)  11.1 us
  transfers between devices with their start and end apart: 7, of which 2 were waited for; matrix products, arithmetic and copies ran while one was open for 6% of the time, Pallas kernels for 0%

commit v1 on v0

--- a/solution.py
+++ b/solution.py
@@ -24,7 +24,9 @@
 def stacked_from(value, axes, sequence):
     tiles = value[None]
     for k in sequence:
-        tiles = lax.all_gather(tiles, axes[k], axis=0, tiled=True)
+        tiles = jnp.concatenate(
+            lax.all_to_all(jnp.stack([tiles] * lax.axis_size(axes[k])), axes[k], 0, 0), axis=0
+        )
     block = [lax.axis_size(axes[k]) for k in reversed(sequence)]
     tiles = tiles.reshape(*block, *value.shape)
     turned = sorted(range(len(sequence)), key=lambda place: sequence[len(sequence) - 1 - place])

time: 475 us -> 261 us (0.55)
  the two profiles are of different devices: /device:TPU:2 before, /device:TPU:4 now
where the time goes in v1:
time: 261 us; the launch traced here: 259 us
  waiting for transfers between devices  91.6 us (35%)
  starting transfers between devices  61.7 us (24%)
  local copies, waits for them, and re-layouts  43.3 us (17%)
  other arithmetic  21.2 us (8%)
  between operations  14.5 us (6%)
  blocking collectives  14.1 us (5%)
  matrix products  12.8 us (5%)
    all_to_all x6, waiting for transfers between devices, stacked_from(): lax.all_to_all(jnp.stack([tiles] * lax.axis_size(axes[k])), axes[k], 0, 0)  50.4 us
    all_to_all x6, starting transfers between devices, stacked_from(): lax.all_to_all(jnp.stack([tiles] * lax.axis_size(axes[k])), axes[k], 0, 0)  44.8 us
    reduce_scatter x1, waiting for transfers between devices, body(): lax.psum_scatter(terms.astype(jnp.bfloat16), 'tp', scatter_dimension=1, t...  37.9 us
    unnamed x83, local copies, waits for them, and re-layouts  17.7 us
    all_to_all x3, blocking collectives, stacked_from(): lax.all_to_all(jnp.stack([tiles] * lax.axis_size(axes[k])), axes[k], 0, 0)  14.1 us
    ppermute x4, starting transfers between devices, shifted(): return lax.ppermute(block, axis, route)  11.2 us
    dot_general x3, matrix products, add_rows(): jnp.dot(columns, piece.reshape(rows, -1), preferred_element_type=jnp.floa...  5.51 us
    another operation x4, other arithmetic, stacked_from(): jnp.stack([tiles] * lax.axis_size(axes[k]))  5.26 us
  transfers between devices with their start and end apart: 13, of which 7 were waited for; matrix products, arithmetic and copies ran while one was open for 24% of the time, Pallas kernels for 0%

profile of v1, /device:TPU:4, one launch (start us, length us, event | category | flops | bytes accessed | tf_op | source)
XLA Modules:
  0.0 259.2 jit_solution(497345787227937397)
XLA Ops:
  7.9 15.2 %all-to-all-start.6 = ((bf16[16,1,128,8]{2,3,1,0:T(8,128)(2,1)}), bf16[16,1,128,8]{2,3,1,0:T(8,128)(2,1)S(1)}, u32[]{:S(2)}, u32[]{:S(2)}) async-start(bf16[16,1,128,8]{2,3,1,0:T(8,128)(2,1)} %stack.50), calls=%async_computation.6 | async-start | bytes 65536 | tf_op jit(solution)/shard_map/all_to_all | solution.py:28
  23.2 1.5 fusion.2
  24.7 1.1 stack.41
  25.9 1.2 reshape.599
  27.5 1.2 reshape.595
  28.8 6.9 %all-to-all-done.6 = bf16[16,1,128,8]{2,3,1,0:T(8,128)(2,1)S(1)} async-done(((bf16[16,1,128,8]{2,3,1,0:T(8,128)(2,1)}), bf16[16,1,128,8]{2,3,1,0:T(8,128)(2,1)S(1)}, u32[]{:S(2)}, u32[]{:S(2)}) %all-to-all-start.6) | async-done | bytes 32800 | tf_op jit(solution)/shard_map/all_to_all | solution.py:28
  36.4 4.8 %all-to-all-start.7 = ((bf16[4,16,128,8]{2,3,1,0:T(8,128)(2,1)}), bf16[4,16,128,8]{2,3,1,0:T(8,128)(2,1)S(1)}, u32[]{:S(2)}, u32[]{:S(2)}) async-start(bf16[4,16,128,8]{2,3,1,0:T(8,128)(2,1)} %stack.51), calls=%async_computation.7 | async-start | bytes 262144 | tf_op jit(solution)/shard_map/all_to_all | solution.py:28
  41.2 3.3 %all-to-all-done.7 = bf16[4,16,128,8]{2,3,1,0:T(8,128)(2,1)S(1)} async-done(((bf16[4,16,128,8]{2,3,1,0:T(8,128)(2,1)}), bf16[4,16,128,8]{2,3,1,0:T(8,128)(2,1)S(1)}, u32[]{:S(2)}, u32[]{:S(2)}) %all-to-all-start.7) | async-done | bytes 131104 | tf_op jit(solution)/shard_map/all_to_all | solution.py:28
  44.4 8.9 %all-to-all-start.2 = ((bf16[64,2,1536]{2,1,0:T(2,128)(2,1)}), bf16[64,2,1536]{2,1,0:T(2,128)(2,1)S(1)}, u32[]{:S(2)}, u32[]{:S(2)}) async-start(bf16[64,2,1536]{2,1,0:T(2,128)(2,1)} %reshape.599), calls=%async_computation.2 | async-start | bytes 786432 | tf_op jit(solution)/shard_map/all_to_all | solution.py:28
  54.6 23.8 %all-to-all-done.2 = bf16[64,2,1536]{2,1,0:T(2,128)(2,1)S(1)} async-done(((bf16[64,2,1536]{2,1,0:T(2,128)(2,1)}), bf16[64,2,1536]{2,1,0:T(2,128)(2,1)S(1)}, u32[]{:S(2)}, u32[]{:S(2)}) %all-to-all-start.2) | async-done | bytes 393248 | tf_op jit(solution)/shard_map/all_to_all | solution.py:28
  78.4 6.0 %all-to-all-start.4 = ((bf16[64,2,1536]{2,1,0:T(2,128)(2,1)}), bf16[64,2,1536]{2,1,0:T(2,128)(2,1)S(1)}, u32[]{:S(2)}, u32[]{:S(2)}) async-start(bf16[64,2,1536]{2,1,0:T(2,128)(2,1)} %reshape.595), calls=%async_computation.4 | async-start | bytes 786432 | tf_op jit(solution)/shard_map/all_to_all | solution.py:28
  84.8 1.2 reshape.603
  88.7 0.7 convert_multiply_fusion.10
  90.6 1.5 pad_maximum_fusion.1
  92.1 1.2 reshape.601
  93.4 16.3 %all-to-all-done.4 = bf16[64,2,1536]{2,1,0:T(2,128)(2,1)S(1)} async-done(((bf16[64,2,1536]{2,1,0:T(2,128)(2,1)}), bf16[64,2,1536]{2,1,0:T(2,128)(2,1)S(1)}, u32[]{:S(2)}, u32[]{:S(2)}) %all-to-all-start.4) | async-done | bytes 393248 | tf_op jit(solution)/shard_map/all_to_all | solution.py:28
  109.7 4.1 %all-to-all-start.8 = ((bf16[2,64,128,8]{2,3,1,0:T(8,128)(2,1)}), bf16[2,64,128,8]{2,3,1,0:T(8,128)(2,1)}, u32[]{:S(2)}, u32[]{:S(2)}) async-start(bf16[2,64,128,8]{2,3,1,0:T(8,128)(2,1)} %pad_maximum_fusion.6), calls=%async_computation.8 | async-start | bytes 524288 | tf_op jit(solution)/shard_map/all_to_all | solution.py:28
  114.3 1.5 pad_maximum_fusion.2
  115.8 2.0 reshape.597
  117.7 4.5 %all_to_all.45 = bf16[2,2,98304]{2,1,0:T(2,128)(2,1)S(1)} all-to-all(bf16[2,2,98304]{2,1,0:T(2,128)(2,1)S(1)} %reshape.601), channel_id=1, replica_groups=mesh['sp_0'=16,'sp_1'=4,'sp_2'=2,'tp'=4] {'sp_2'}, dimensions={0} | all-to-all | bytes 1572864 | tf_op jit(solution)/shard_map/all_to_all | solution.py:28
  122.3 5.3 %all_to_all.46 = bf16[2,2,98304]{2,1,0:T(2,128)(2,1)} all-to-all(bf16[2,2,98304]{2,1,0:T(2,128)(2,1)S(1)} %copy-done.1), channel_id=1, replica_groups=mesh['sp_0'=16,'sp_1'=4,'sp_2'=2,'tp'=4] {'sp_2'}, dimensions={0} | all-to-all | bytes 1572864 | tf_op jit(solution)/shard_map/all_to_all | solution.py:28
  127.5 6.0 %all-to-all-start = ((bf16[64,2,1536]{2,1,0:T(2,128)(2,1)}), bf16[64,2,1536]{2,1,0:T(2,128)(2,1)S(1)}, u32[]{:S(2)}, u32[]{:S(2)}) async-start(bf16[64,2,1536]{2,1,0:T(2,128)(2,1)} %reshape.603), calls=%async_computation | async-start | bytes 786432 | tf_op jit(solution)/shard_map/all_to_all | solution.py:28
  134.1 0.7 broadcast_multiply_fusion
  134.9 1.3 fusion.4
  136.1 1.7 copy.197
  137.9 1.0 reshape.602
  138.9 1.1 copy.156
  140.0 1.7 reshape_reshape_reshape.10
  141.7 2.2 reshape.598
  143.9 1.1 copy.158
  145.0 1.7 reshape_reshape_reshape.11
  146.7 1.8 convolution_convert_fusion.2
  148.9 1.0 copy.160
  150.0 1.8 convolution_convert_fusion.1
  152.2 1.0 copy.161
  153.2 0.9 fusion.57
  154.1 2.5 collective-permute-start.5
  156.6 3.4 %collective-permute-start.4 = (bf16[4,128,2,128]{1,3,2,0:T(8,128)(2,1)}, bf16[4,128,2,128]{1,3,2,0:T(8,128)(2,1)}, u32[]{:S(2)}, u32[]{:S(2)}) collective-permute-start(bf16[4,128,2,128]{1,3,2,0:T(8,128)(2,1)} %get-tuple-element.13), channel_id=1, source_target_pairs={{0,8},{4,12},{8,16},{12,20},{16,24},{20,28},{24,32},{28,36},{32,40... | collective-permute-start | bytes 786440 | tf_op jit(solution)/shard_map/ppermute | solution.py:65
  159.9 0.8 fusion.43
  161.4 1.5 pad_maximum_fusion
  162.9 1.2 reshape.605
  164.1 4.4 %all_to_all.47 = bf16[2,2,98304]{2,1,0:T(2,128)(2,1)S(1)} all-to-all(bf16[2,2,98304]{2,1,0:T(2,128)(2,1)S(1)} %reshape.605), channel_id=1, replica_groups=mesh['sp_0'=16,'sp_1'=4,'sp_2'=2,'tp'=4] {'sp_2'}, dimensions={0} | all-to-all | bytes 1572864 | tf_op jit(solution)/shard_map/all_to_all | solution.py:28
  168.5 1.0 reshape.606
  169.5 1.1 copy.154
  170.6 1.7 reshape_reshape_reshape.9
  172.3 1.8 convolution_convert_fusion.3
  175.7 2.1 collective-permute-start
  177.9 3.4 %collective-permute-start.1 = (bf16[4,32,2,128]{1,3,2,0:T(8,128)(2,1)S(1)}, bf16[4,32,2,128]{1,3,2,0:T(8,128)(2,1)S(1)}, u32[]{:S(2)}, u32[]{:S(2)}) collective-permute-start(bf16[4,32,2,128]{1,3,2,0:T(8,128)(2,1)S(1)} %get-tuple-element.21), channel_id=1, source_target_pairs={{4,0},{8,4},{12,8},{16,12},{20,16},{24,20},{28,24},{32,28},{36,32}... | collective-permute-start | bytes 196616 | tf_op jit(solution)/shard_map/ppermute | solution.py:55
  181.3 1.9 collective-permute-start.3
  183.3 1.0 multiply_multiply_fusion.1
  184.3 0.9 multiply_multiply_fusion
  185.3 3.5 %collective-permute-start.2 = (bf16[4,128,2,2,128]{1,4,3,0,2:T(8,128)(2,1)S(1)}, bf16[4,128,2,2,128]{1,4,3,0,2:T(8,128)(2,1)S(1)}, u32[]{:S(2)}, u32[]{:S(2)}) collective-permute-start(bf16[4,128,2,2,128]{1,4,3,0,2:T(8,128)(2,1)S(1)} %copy-done.10), channel_id=1, source_target_pairs={{0,4},{4,8},{8,12},{12,16},{16,20},{20,24},{24,28},{28,32},{32,36}... | collective-permute-start | bytes 1572872 | tf_op jit(solution)/shard_map/ppermute | solution.py:65
  190.4 1.0 convolution_bitcast_fusion.1
  191.4 1.0 constant_dynamic-update-slice_fusion.2
  192.5 3.3 %collective-permute-done.2 = bf16[4,128,2,2,128]{1,4,3,0,2:T(8,128)(2,1)S(1)} collective-permute-done((bf16[4,128,2,2,128]{1,4,3,0,2:T(8,128)(2,1)S(1)}, bf16[4,128,2,2,128]{1,4,3,0,2:T(8,128)(2,1)S(1)}, u32[]{:S(2)}, u32[]{:S(2)}) %collective-permute-start.2) | collective-permute-done | bytes 524320 | tf_op jit(solution)/shard_map/ppermute | solution.py:65
  197.0 1.6 fusion.94
  199.8 1.0 constant_dynamic-update-slice_fusion.1
  201.8 1.0 constant_dynamic-update-slice_fusion
  203.3 0.8 copy.176
  204.1 1.9 fusion.93
  208.1 0.7 copy.186
  210.5 0.8 copy.189
  213.0 1.4 convolution_convert_fusion
  214.4 37.9 %reduce-scatter.2.cloned.1.call-done = bf16[512,256]{1,0:T(8,128)(2,1)} async-done(((bf16[512,1024]{1,0:T(8,128)(2,1)}), bf16[512,256]{1,0:T(8,128)(2,1)}) %reduce-scatter.2.cloned.1.call-update) | async-done | bytes 262160 | tf_op jit(solution)/shard_map/reduce_scatter | solution.py:205
  (171 shorter events, 22.7 us)
Async XLA Ops:
  7.9 27.8 %all-to-all-start.6 = ((bf16[16,1,128,8]{2,3,1,0:T(8,128)(2,1)}), bf16[16,1,128,8]{2,3,1,0:T(8,128)(2,1)S(1)}, u32[]{:S(2)}, u32[]{:S(2)}) async-start(bf16[16,1,128,8]{2,3,1,0:T(8,128)(2,1)} %stack.50), calls=%async_computation.6 | async-start | bytes 65536 | tf_op jit(solution)/shard_map/all_to_all | solution.py:28
  23.2 3.9 %copy-start.24 = (bf16[8,3,2,64]{3,2,1,0:T(2,128)(2,1)S(1)}, bf16[8,3,2,64]{3,2,1,0:T(2,128)(2,1)}, u32[]{:S(2)}) copy-start(bf16[8,3,2,64]{3,2,1,0:T(2,128)(2,1)} %param.12) | copy-start | bytes 18436
  27.5 25.8 %copy-start.30 = (f32[3,64]{1,0:T(4,128)S(1)}, f32[3,64]{1,0:T(4,128)}, u32[]{:S(2)}) copy-start(f32[3,64]{1,0:T(4,128)} %param.13) | copy-start | bytes 2308
  28.8 55.6 %copy-start.25 = (bf16[8,3,2,64]{3,2,1,0:T(2,128)(2,1)S(1)}, bf16[8,3,2,64]{3,2,1,0:T(2,128)(2,1)}, u32[]{:S(2)}) copy-start(bf16[8,3,2,64]{3,2,1,0:T(2,128)(2,1)} %param.10) | copy-start | bytes 18436
  36.4 8.1 %all-to-all-start.7 = ((bf16[4,16,128,8]{2,3,1,0:T(8,128)(2,1)}), bf16[4,16,128,8]{2,3,1,0:T(8,128)(2,1)S(1)}, u32[]{:S(2)}, u32[]{:S(2)}) async-start(bf16[4,16,128,8]{2,3,1,0:T(8,128)(2,1)} %stack.51), calls=%async_computation.7 | async-start | bytes 262144 | tf_op jit(solution)/shard_map/all_to_all | solution.py:28
  44.4 34.0 %all-to-all-start.2 = ((bf16[64,2,1536]{2,1,0:T(2,128)(2,1)}), bf16[64,2,1536]{2,1,0:T(2,128)(2,1)S(1)}, u32[]{:S(2)}, u32[]{:S(2)}) async-start(bf16[64,2,1536]{2,1,0:T(2,128)(2,1)} %reshape.599), calls=%async_computation.2 | async-start | bytes 786432 | tf_op jit(solution)/shard_map/all_to_all | solution.py:28
  78.4 31.2 %all-to-all-start.4 = ((bf16[64,2,1536]{2,1,0:T(2,128)(2,1)}), bf16[64,2,1536]{2,1,0:T(2,128)(2,1)S(1)}, u32[]{:S(2)}, u32[]{:S(2)}) async-start(bf16[64,2,1536]{2,1,0:T(2,128)(2,1)} %reshape.595), calls=%async_computation.4 | async-start | bytes 786432 | tf_op jit(solution)/shard_map/all_to_all | solution.py:28
  109.7 8.1 %all-to-all-start.8 = ((bf16[2,64,128,8]{2,3,1,0:T(8,128)(2,1)}), bf16[2,64,128,8]{2,3,1,0:T(8,128)(2,1)}, u32[]{:S(2)}, u32[]{:S(2)}) async-start(bf16[2,64,128,8]{2,3,1,0:T(8,128)(2,1)} %pad_maximum_fusion.6), calls=%async_computation.8 | async-start | bytes 524288 | tf_op jit(solution)/shard_map/all_to_all | solution.py:28
  117.7 4.5 %copy-start.1 = (bf16[2,2,98304]{2,1,0:T(2,128)(2,1)S(1)}, bf16[2,2,98304]{2,1,0:T(2,128)(2,1)}, u32[]{:S(2)}) copy-start(bf16[2,2,98304]{2,1,0:T(2,128)(2,1)} %reshape.597) | copy-start | bytes 2359300
  122.2 11.3 %copy-start.31 = (f32[3,64]{1,0:T(4,128)S(1)}, f32[3,64]{1,0:T(4,128)}, u32[]{:S(2)}) copy-start(f32[3,64]{1,0:T(4,128)} %param.14) | copy-start | bytes 2308
  122.2 11.9 %copy-start.15 = (f32[128,192]{0,1:T(8,128)S(1)}, f32[128,192]{0,1:T(8,128)}, u32[]{:S(2)}) copy-start(f32[128,192]{0,1:T(8,128)} %convert_multiply_fusion.10) | copy-start | bytes 294916
  122.2 12.6 %copy-start = (bf16[4,128,1024]{2,1,0:T(8,128)(2,1)S(1)}, bf16[4,128,1024]{2,1,0:T(8,128)(2,1)}, u32[]{:S(2)}) copy-start(bf16[4,128,1024]{2,1,0:T(8,128)(2,1)} %param.8) | copy-start | bytes 3145732
  122.2 12.6 %copy-start.26 = (f32[1024]{0:T(1024)S(1)}, f32[1024]{0:T(1024)}, u32[]{:S(2)}) copy-start(f32[1024]{0:T(1024)} %param.9) | copy-start | bytes 12292
  127.5 33.4 %all-to-all-start = ((bf16[64,2,1536]{2,1,0:T(2,128)(2,1)}), bf16[64,2,1536]{2,1,0:T(2,128)(2,1)S(1)}, u32[]{:S(2)}, u32[]{:S(2)}) async-start(bf16[64,2,1536]{2,1,0:T(2,128)(2,1)} %reshape.603), calls=%async_computation | async-start | bytes 786432 | tf_op jit(solution)/shard_map/all_to_all | solution.py:28
  133.5 118.8 %reduce-scatter.2.cloned.1.call-start = ((), (), s32[]{:S(2)}) async-start(), calls=%async_computation.10 | async-start | bytes 1310720 | tf_op jit(solution)/shard_map/reduce_scatter | solution.py:205
  145.0 1.7 copy-start.3
  148.5 1.4 copy-start.4
  154.1 47.7 %collective-permute-start.5 = (bf16[4,128,2,128]{1,3,2,0:T(8,128)(2,1)}, bf16[4,128,2,128]{1,3,2,0:T(8,128)(2,1)}, u32[]{:S(2)}, u32[]{:S(2)}) collective-permute-start(bf16[4,128,2,128]{1,3,2,0:T(8,128)(2,1)} %get-tuple-element.13), channel_id=1, source_target_pairs={{8,0},{12,4},{16,8},{20,12},{24,16},{28,20},{32,24},{36,28},{40,32... | collective-permute-start | bytes 786440 | tf_op jit(solution)/shard_map/ppermute | solution.py:65
  156.6 34.9 %collective-permute-start.4 = (bf16[4,128,2,128]{1,3,2,0:T(8,128)(2,1)}, bf16[4,128,2,128]{1,3,2,0:T(8,128)(2,1)}, u32[]{:S(2)}, u32[]{:S(2)}) collective-permute-start(bf16[4,128,2,128]{1,3,2,0:T(8,128)(2,1)} %get-tuple-element.13), channel_id=1, source_target_pairs={{0,8},{4,12},{8,16},{12,20},{16,24},{20,28},{24,32},{28,36},{32,40... | collective-permute-start | bytes 786440 | tf_op jit(solution)/shard_map/ppermute | solution.py:65
  170.6 1.7 copy-start.5
  174.2 0.8 copy-start.27
  175.1 6.2 %copy-start.10 = (bf16[4,128,2,2,128]{1,4,3,0,2:T(8,128)(2,1)S(1)}, bf16[4,128,2,2,128]{1,4,3,0,2:T(8,128)(2,1)}, u32[]{:S(2)}) copy-start(bf16[4,128,2,2,128]{1,4,3,0,2:T(8,128)(2,1)} %fusion.43) | copy-start | bytes 1572868
  175.4 9.0 %copy-start.28 = (f32[64]{0:T(128)S(1)}, f32[64]{0:T(128)}, u32[]{:S(2)}) copy-start(f32[64]{0:T(128)} %get-tuple-element.26) | copy-start | bytes 772
  175.7 9.5 %collective-permute-start = (bf16[4,32,2,128]{1,3,2,0:T(8,128)(2,1)S(1)}, bf16[4,32,2,128]{1,3,2,0:T(8,128)(2,1)S(1)}, u32[]{:S(2)}, u32[]{:S(2)}) collective-permute-start(bf16[4,32,2,128]{1,3,2,0:T(8,128)(2,1)S(1)} %get-tuple-element.20), channel_id=1, source_target_pairs={{0,4},{4,8},{8,12},{12,16},{16,20},{20,24},{24,28},{28,32},{32,36}... | collective-permute-start | bytes 196616 | tf_op jit(solution)/shard_map/ppermute | solution.py:53
  177.9 10.8 %collective-permute-start.1 = (bf16[4,32,2,128]{1,3,2,0:T(8,128)(2,1)S(1)}, bf16[4,32,2,128]{1,3,2,0:T(8,128)(2,1)S(1)}, u32[]{:S(2)}, u32[]{:S(2)}) collective-permute-start(bf16[4,32,2,128]{1,3,2,0:T(8,128)(2,1)S(1)} %get-tuple-element.21), channel_id=1, source_target_pairs={{4,0},{8,4},{12,8},{16,12},{20,16},{24,20},{28,24},{32,28},{36,32}... | collective-permute-start | bytes 196616 | tf_op jit(solution)/shard_map/ppermute | solution.py:55
  181.3 11.1 %collective-permute-start.3 = (bf16[4,128,2,2,128]{1,4,3,0,2:T(8,128)(2,1)S(1)}, bf16[4,128,2,2,128]{1,4,3,0,2:T(8,128)(2,1)S(1)}, u32[]{:S(2)}, u32[]{:S(2)}) collective-permute-start(bf16[4,128,2,2,128]{1,4,3,0,2:T(8,128)(2,1)S(1)} %copy-done.10), channel_id=1, source_target_pairs={{4,0},{8,4},{12,8},{16,12},{20,16},{24,20},{28,24},{32,28},{36,32}... | collective-permute-start | bytes 1572872 | tf_op jit(solution)/shard_map/ppermute | solution.py:65
  184.3 4.9 %copy-start.16 = (f32[2,128,192]{1,2,0:T(8,128)S(1)}, f32[2,128,192]{1,2,0:T(8,128)}, u32[]{:S(2)}) copy-start(f32[2,128,192]{1,2,0:T(8,128)} %broadcast_multiply_fusion) | copy-start | bytes 589828
  184.3 4.9 %copy-start.19 = (pred[128,192]{0,1:T(8,128)(4,1)S(1)}, pred[128,192]{0,1:T(8,128)(4,1)}, u32[]{:S(2)}) copy-start(pred[128,192]{0,1:T(8,128)(4,1)} %fusion.71) | copy-start | bytes 73732
  184.3 4.9 %copy-start.32 = (f32[64]{0:T(128)S(1)}, f32[64]{0:T(128)}, u32[]{:S(2)}) copy-start(f32[64]{0:T(128)} %get-tuple-element.22) | copy-start | bytes 772
  185.3 10.5 %collective-permute-start.2 = (bf16[4,128,2,2,128]{1,4,3,0,2:T(8,128)(2,1)S(1)}, bf16[4,128,2,2,128]{1,4,3,0,2:T(8,128)(2,1)S(1)}, u32[]{:S(2)}, u32[]{:S(2)}) collective-permute-start(bf16[4,128,2,2,128]{1,4,3,0,2:T(8,128)(2,1)S(1)} %copy-done.10), channel_id=1, source_target_pairs={{0,4},{4,8},{8,12},{12,16},{16,20},{20,24},{24,28},{28,32},{32,36}... | collective-permute-start | bytes 1572872 | tf_op jit(solution)/shard_map/ppermute | solution.py:65
  190.4 5.4 %copy-start.7 = (bf16[4,128,2,128]{1,3,2,0:T(8,128)(2,1)S(1)}, bf16[4,128,2,128]{1,3,2,0:T(8,128)(2,1)}, u32[]{:S(2)}) copy-start(bf16[4,128,2,128]{1,3,2,0:T(8,128)(2,1)} %get-tuple-element.14) | copy-start | bytes 786436
  192.4 3.5 %copy-start.11 = (bf16[4,128,2,2,128]{1,4,3,0,2:T(8,128)(2,1)}, bf16[4,128,2,2,128]{1,4,3,0,2:T(8,128)(2,1)S(1)}, u32[]{:S(2)}) copy-start(bf16[4,128,2,2,128]{1,4,3,0,2:T(8,128)(2,1)S(1)} %collective-permute-done.3) | copy-start | bytes 1572868
  195.7 0.8 copy-start.13
  196.0 0.9 copy-start.18
  196.0 0.9 copy-start.20
  196.9 2.8 %copy-start.14 = (bf16[4,128,2,2,128]{1,4,3,0,2:T(8,128)(2,1)S(1)}, bf16[4,128,2,2,128]{1,4,3,0,2:T(8,128)(2,1)}, u32[]{:S(2)}) copy-start(bf16[4,128,2,2,128]{1,4,3,0,2:T(8,128)(2,1)} %copy-done.13) | copy-start | bytes 1572868
  198.6 3.2 %copy-start.12 = (bf16[4,128,2,2,128]{1,4,3,0,2:T(8,128)(2,1)S(1)}, bf16[4,128,2,2,128]{1,4,3,0,2:T(8,128)(2,1)}, u32[]{:S(2)}) copy-start(bf16[4,128,2,2,128]{1,4,3,0,2:T(8,128)(2,1)} %copy-done.11) | copy-start | bytes 1572868
  199.8 3.3 %copy-start.29 = (f32[64]{0:T(128)S(1)}, f32[64]{0:T(128)}, u32[]{:S(2)}) copy-start(f32[64]{0:T(128)} %get-tuple-element.23) | copy-start | bytes 772
  206.0 3.6 %copy-start.8 = (f32[4,16,2,8,40]{4,3,2,1,0:T(8,128)}, f32[4,16,2,8,40]{4,3,2,1,0:T(8,128)S(1)}, u32[]{:S(2)}) copy-start(f32[4,16,2,8,40]{4,3,2,1,0:T(8,128)S(1)} %get-tuple-element.29) | copy-start | bytes 491524
  209.6 0.8 copy-start.17
  210.0 1.3 copy-start.9
  211.8 0.7 copy-start.21
  211.8 0.7 copy-start.22
  211.8 0.7 copy-start.23
  211.8 1.0 copy-start.2
  211.8 1.1 copy-start.6
Sparse Core Ops, SparseCore 0:
  214.5 37.7 reduce-scatter.1
